TPU v7x, 32 devices: a whole 2x2x4 slice. The times are simulated.
32 devices in a mesh: sp: 8 (over z, x), tp: 4 (over y, core).
Axes of the slice: x: 2, y: 2, z: 4, core: 2. Of those that a mesh axis runs over, the one named last changes fastest.
Arguments:
- queries: bfloat16 [512, 16, 192], P('sp', 'tp'), may hold values from -400 to 400
- latents: bfloat16 [512, 512], P('sp'), may hold values from -6 to 6
- rope_keys: bfloat16 [512, 64], P('sp'), may hold values from -9 to 9
- latent_norm_scale: float32 [512], replicated, may hold values from 0.1 to 1.9
- key_value_weight: bfloat16 [512, 16, 256], P(None, 'tp'), may hold values from -0.25 to 0.25
- out_weight: bfloat16 [2048, 2048], P('tp'), may hold values from -1 to 1
- resid: bfloat16 [512, 2048], P('sp'), may hold values from -3 to 3
- ffn_gain: float32 [2048], replicated, may hold values from 0.1 to 1.9
- expert_ids: int32 [512, 2], P('sp'), may hold values from 0 to 7, all different within a row; in each aligned block of 64 rows (0 to 63, 64 to 127, ...) at most 24 rows name the same one
- route_weights: float32 [512, 2], P('sp'), may hold values from 0.1 to 1
- gate_weight: bfloat16 [8, 2048, 4096], P('sp', None, 'tp'), may hold values from -0.125 to 0.125
- up_weight: bfloat16 [8, 2048, 4096], P('sp', None, 'tp'), may hold values from -0.125 to 0.125
- down_weight: bfloat16 [8, 4096, 2048], P('sp', 'tp'), may hold values from -0.09375 to 0.09375
Outputs:
- updated: bfloat16 [512, 2048], P('sp', 'tp')
Inputs may be any that keep to these rules, and one draw needn't show every extreme that they name: `expert_ids`: among the rows of one device no expert is named more than 24 times, and in some devices some expert is named exactly 24 times.
All inputs are finite; a program needn't handle non-finite values.
Results may differ from a plain program's by a relative error of at most 0.025.
Values may be sent and summed in bfloat16 or wider, within the bound.
A program may use at most 64 MiB of HBM per device.

v0:
```python
import jax
import jax.numpy as jnp
from jax import lax
from jax.sharding import PartitionSpec as P

PLAIN_WIDTH = 128
VALUE_WIDTH = 128
rope_base = 10000.0
norm_eps = 1e-06


def rotary_table(positions, width):
    half_width = width // 2
    inverse = rope_base ** (-jnp.arange(half_width, dtype=jnp.float32) / half_width)
    turned = positions[:, None] * inverse[None, :]
    return (jnp.cos(turned), jnp.sin(turned))


def turn_pairs(vectors, cosines, sines):
    half_width = vectors.shape[-1] // 2
    front_half = vectors[..., :half_width]
    back_half = vectors[..., half_width:]
    return jnp.concatenate(
        [front_half * cosines - back_half * sines, back_half * cosines + front_half * sines],
        axis=-1,
    )


def rms_scaled(matrix, gain):
    floats = matrix.astype(jnp.float32)
    return floats * lax.rsqrt(jnp.mean(floats * floats, axis=-1, keepdims=True) + norm_eps) * gain


def attend(state_now, query_plain, query_turned, key_plain, key_turned, head_values):
    running, totals, accumulated = state_now
    score_scale = (query_plain.shape[-1] + query_turned.shape[-1]) ** (-0.5)
    scores = jnp.einsum("qhn,khn->hqk", query_plain, key_plain, preferred_element_type=jnp.float32)
    scores = (
        scores
        + jnp.einsum("qhr,kr->hqk", query_turned, key_turned, preferred_element_type=jnp.float32)
    ) * score_scale
    highest = jnp.max(scores, axis=-1)
    fade_by = jnp.exp(running - highest)
    exps = jnp.exp(scores - highest[..., None])
    totals = totals * fade_by + jnp.sum(exps, axis=-1)
    summed = jnp.einsum(
        "hqk,khv->qhv", exps.astype(jnp.bfloat16), head_values, preferred_element_type=jnp.float32
    )
    accumulated = accumulated * jnp.transpose(fade_by)[:, :, None] + summed
    return (highest, totals, accumulated)


def finish_expert(gate_act, up_act, down_matrix, senders, items):
    hidden = (jax.nn.silu(gate_act) * up_act).astype(jnp.bfloat16)
    partial_rows = jnp.dot(hidden, down_matrix, preferred_element_type=jnp.float32).reshape(
        senders, items, -1
    )
    col_share = lax.psum_scatter(
        partial_rows.astype(jnp.bfloat16), "tp", scatter_dimension=2, tiled=True
    )
    return lax.all_to_all(col_share, "sp", split_axis=0, concat_axis=0, tiled=True)


def shards(
    queries,
    latents,
    rope_keys,
    latent_norm_scale,
    key_value_weight,
    out_weight,
    resid,
    ffn_gain,
    expert_ids,
    route_weights,
    gate_weight,
    up_weight,
    down_weight,
):
    tok_rows, local_heads, _ = queries.shape
    offset = lax.axis_index("sp") * tok_rows
    positions = (offset + jnp.arange(tok_rows, dtype=jnp.int32)).astype(jnp.float32)
    cosines, sines = rotary_table(positions, rope_keys.shape[1])
    query_plain = queries[:, :, :PLAIN_WIDTH]
    query_turned = turn_pairs(
        queries[:, :, PLAIN_WIDTH:].astype(jnp.float32), cosines[:, None, :], sines[:, None, :]
    ).astype(jnp.bfloat16)
    key_turned = turn_pairs(rope_keys.astype(jnp.float32), cosines, sines).astype(jnp.bfloat16)
    normalized_latent = rms_scaled(latents, latent_norm_scale).astype(jnp.bfloat16)
    key_project = key_value_weight.reshape(key_value_weight.shape[0], -1)
    pair_rows = tok_rows // 2
    turned_pairs = key_turned.reshape(pair_rows, -1)
    start_state = (
        jnp.full((local_heads, tok_rows), -jnp.inf, jnp.float32),
        jnp.zeros((local_heads, tok_rows), jnp.float32),
        jnp.zeros((tok_rows, local_heads, VALUE_WIDTH), jnp.float32),
    )
    own_projected = jnp.dot(
        normalized_latent, key_project, preferred_element_type=jnp.float32
    ).astype(jnp.bfloat16)
    head_piece = lax.all_gather(own_projected.reshape(pair_rows, -1), "sp", axis=0, tiled=True)
    turned_piece = lax.all_gather(turned_pairs, "sp", axis=0, tiled=True)
    row_count = head_piece.shape[0] * 2
    projected_rows = head_piece.reshape(row_count, -1)
    per_head = projected_rows.reshape(row_count, local_heads, -1)
    key_plain = per_head[:, :, :PLAIN_WIDTH]
    head_values = per_head[:, :, PLAIN_WIDTH:]
    final_state = attend(
        start_state,
        query_plain,
        query_turned,
        key_plain,
        turned_piece.reshape(row_count, -1),
        head_values,
    )
    _, totals, accumulated = final_state
    attended = (accumulated / jnp.transpose(totals)[:, :, None]).astype(jnp.bfloat16)
    head_partial = jnp.dot(
        attended.reshape(tok_rows, -1), out_weight, preferred_element_type=jnp.float32
    )
    mixed = lax.psum(head_partial.astype(jnp.bfloat16), "tp").astype(jnp.float32)
    middle_float = (resid.astype(jnp.float32) + mixed).astype(jnp.bfloat16).astype(jnp.float32)
    normed = rms_scaled(middle_float, ffn_gain).astype(jnp.bfloat16)
    experts = lax.axis_size("sp")
    top_count = expert_ids.shape[1]
    capacity = (3 * tok_rows * top_count + 2 * experts - 1) // (2 * experts)
    flat_ids = expert_ids.reshape(-1)
    picked = (flat_ids[:, None] == jnp.arange(experts, dtype=jnp.int32)[None, :]).astype(jnp.int32)
    slot_rank = jnp.sum((jnp.cumsum(picked, axis=0) - picked) * picked, axis=1)
    slot_index = flat_ids * capacity + slot_rank
    sources = jnp.arange(flat_ids.shape[0], dtype=jnp.int32) // top_count
    owner_row = jnp.zeros((experts * capacity,), jnp.int32).at[slot_index].set(sources)
    filled = jnp.zeros((experts * capacity,), jnp.bool_).at[slot_index].set(True)
    outgoing = jnp.where(filled[:, None], normed[owner_row], jnp.zeros((), jnp.bfloat16)).reshape(
        experts, capacity, -1
    )
    arrived = lax.all_to_all(outgoing, "sp", split_axis=0, concat_axis=0, tiled=True)
    senders, items, width = arrived.shape
    rows_in = arrived.reshape(-1, width)
    gate_act = jnp.dot(rows_in, gate_weight[0], preferred_element_type=jnp.float32)
    up_act = jnp.dot(rows_in, up_weight[0], preferred_element_type=jnp.float32)
    returned = finish_expert(gate_act, up_act, down_weight[0], senders, items)
    columns = returned.shape[2]
    back_rows = returned.reshape(-1, columns)
    chosen_rows = back_rows[slot_index].astype(jnp.float32) * route_weights.reshape(-1)[:, None]
    routed = jnp.sum(chosen_rows.reshape(tok_rows, top_count, columns), axis=1)
    column_start = lax.axis_index("tp") * columns
    middle_cols = lax.dynamic_slice_in_dim(middle_float, column_start, columns, 1)
    return (middle_cols + routed).astype(jnp.bfloat16)


def solution(mesh):
    placed = (
        P("sp", "tp", None),
        P("sp", None),
        P("sp", None),
        P(),
        P(None, "tp", None),
        P("tp", None),
        P("sp", None),
        P(),
        P("sp", None),
        P("sp", None),
        P("sp", None, "tp"),
        P("sp", None, "tp"),
        P("sp", "tp", None),
    )
    return jax.shard_map(
        shards, mesh=mesh, in_specs=placed, out_specs=P("sp", "tp"), check_vma=False
    )
```

profile of v0, /device:TPU:0, one launch (start us, length us, event | category | flops | bytes accessed | tf_op | source)
XLA Modules:
  0.0 172.7 jit_solution(10261434299274544389)
XLA Ops:
  6.5 0.0 copy-start
  6.5 0.0 all-gather.2.cloned.1.call-start
  6.5 1.6 copy.35
  8.2 1.0 fusion.28
  9.1 1.2 convolution_convert_fusion.1
  10.3 0.7 reshape.151
  11.0 0.0 all-gather.2.cloned.1.call-update
  11.0 0.0 all-reduce.2.cloned.1.call-start
  11.1 1.5 slice.25
  12.6 0.7 convert_element_type.75
  13.3 0.2 multiply_cosine_fusion
  13.5 0.1 pad_maximum_fusion
  13.6 0.1 convert_element_type.77
  13.7 32.5 %all_gather.7 = bf16[256,128]{1,0:T(8,128)(2,1)S(1)} all-gather(bf16[32,128]{1,0:T(8,128)(2,1)S(1)} %convert_element_type.77), channel_id=1, replica_groups=mesh['sp'=8,'tp'=4] {'sp'}, dimensions={0}, use_global_device_ids=true | all-gather | bytes 73728 | tf_op jit(solution)/shard_map/all_gather | solution.py:101
  46.2 0.1 reshape.152
  46.3 0.0 copy-done.3
  46.3 0.1 copy.26
  46.4 0.1 eq.15
  46.6 0.1 copy.25
  46.7 0.1 mul.175
  46.8 0.1 fusion.39
  46.9 0.2 reduce_window_sum.11
  47.1 0.2 select_reduce_fusion
  47.3 1.0 scatter_custom_fusion.1
  48.2 0.0 slice-done
  48.3 0.8 subtract_convert_fusion
  49.0 5.2 %all-gather.2.cloned.1.call-done = bf16[256,2048]{1,0:T(8,128)(2,1)} async-done(((bf16[32,2048]{1,0:T(8,128)(2,1)}), bf16[256,2048]{1,0:T(8,128)(2,1)}) %all-gather.2.cloned.1.call-update) | async-done | bytes 1048592 | tf_op jit(solution)/shard_map/all_gather | solution.py:100
  54.2 1.8 %reshape_reshape.3 = bf16[512,4,256]{2,1,0:T(4,128)(2,1)S(1)} reshape(bf16[256,2048]{1,0:T(8,128)(2,1)} %all-gather.2.cloned.1.call-done) | data formatting | bytes 2097152 | tf_op jit(solution)/shard_map/reshape;reshape | solution.py:104
  56.1 0.0 copy-start.1
  56.1 0.4 fusion.48
  56.5 0.0 copy-start.2
  56.5 1.1 convolution_bitcast_fusion.1
  57.6 1.2 fusion.49
  58.9 0.2 fusion.23
  59.1 0.3 fusion.20
  59.4 0.0 copy-done
  59.4 1.2 convolution_convert_fusion
  60.6 0.0 all-reduce.2.cloned.1.call-update
  60.6 0.0 reduce-scatter.2.cloned.1.call-start
  60.7 1.0 scatter_custom_fusion
  61.7 0.1 broadcast_in_dim.24
  61.8 29.9 %all-reduce.2.cloned.1.call-done = bf16[64,2048]{1,0:T(8,128)(2,1)} async-done(((bf16[64,2048]{1,0:T(8,128)(2,1)}), bf16[64,2048]{1,0:T(8,128)(2,1)}) %all-reduce.2.cloned.1.call-update) | async-done | bytes 262160 | tf_op jit(solution)/shard_map/psum | solution.py:120
  91.7 1.9 %fusion.26 = (f32[64,2048]{1,0:T(8,128)}, f32[64]{0:T(128)S(1)}) fusion(bf16[64,2048]{1,0:T(8,128)(2,1)} %all-reduce.2.cloned.1.call-done, bf16[64,2048]{1,0:T(8,128)(2,1)S(1)} %copy-done.1), kind=kLoop, calls=%fused_computation.33 | loop fusion | flops 917440 | bytes 1048832 | tf_op jit(solution)/shard_map/convert_element_type | solution.py:121
  93.7 1.1 multiply_convert_fusion
  94.8 1.1 gather_fusion
  95.9 0.0 copy-start.5
  95.9 0.1 broadcast_select_fusion
  96.1 24.6 %all_to_all.10 = bf16[8,24,2048]{2,1,0:T(8,128)(2,1)S(1)} all-to-all(bf16[8,24,2048]{2,1,0:T(8,128)(2,1)S(1)} %broadcast_select_fusion), channel_id=1, replica_groups=mesh['sp'=8,'tp'=4] {'sp'}, dimensions={0} | all-to-all | bytes 1572864 | tf_op jit(solution)/shard_map/all_to_all | solution.py:136
  120.6 3.2 %fusion.4 = f32[192,1024]{1,0:T(8,128)S(1)} fusion(bf16[192,2048]{1,0:T(8,128)(2,1)S(1)} %bitcast.69, bf16[1,2048,1024]{2,1,0:T(8,128)(2,1)} %param.23), kind=kOutput, calls=%fused_computation.8 | convolution fusion | flops 805306368 | bytes 5767168 | tf_op jit(solution)/shard_map/dot_general | solution.py:139
  123.8 0.0 copy-start.6
  123.9 1.1 fusion.12
  124.9 0.0 copy-start.4
  124.9 1.1 copy-done.6
  126.0 1.9 %fusion.6 = bf16[8,24,2048]{2,1,0:T(8,128)(2,1)} fusion(bf16[8,24,1024]{2,1,0:T(8,128)(2,1)S(1)} %bitcast.73, bf16[1,1024,2048]{2,1,0:T(8,128)(2,1)S(1)} %copy-done.6), kind=kOutput, calls=%fused_computation.10 | convolution fusion | flops 805699584 | bytes 5373952 | tf_op jit(solution)/shard_map/dot_general | solution.py:55
  127.9 0.0 reduce-scatter.2.cloned.1.call-update
  128.0 22.0 %reduce-scatter.2.cloned.1.call-done = bf16[8,24,512]{2,1,0:T(8,128)(2,1)} async-done(((bf16[8,24,2048]{2,1,0:T(8,128)(2,1)}), bf16[8,24,512]{2,1,0:T(8,128)(2,1)}) %reduce-scatter.2.cloned.1.call-update) | async-done | bytes 196624 | tf_op jit(solution)/shard_map/reduce_scatter | solution.py:58
  149.9 5.5 %all-to-all-start.1 = ((bf16[8,24,512]{2,1,0:T(8,128)(2,1)}), bf16[8,24,512]{2,1,0:T(8,128)(2,1)S(1)}, u32[]{:S(2)}, u32[]{:S(2)}) async-start(bf16[8,24,512]{2,1,0:T(8,128)(2,1)} %reduce-scatter.2.cloned.1.call-done), calls=%async_computation.2 | async-start | bytes 393216 | tf_op jit(solution)/shard_map/all_to_all | solution.py:61
  155.4 0.0 copy-done.4
  155.4 0.1 copy.27
  155.5 7.7 %all-to-all-done.1 = bf16[8,24,512]{2,1,0:T(8,128)(2,1)S(1)} async-done(((bf16[8,24,512]{2,1,0:T(8,128)(2,1)}), bf16[8,24,512]{2,1,0:T(8,128)(2,1)S(1)}, u32[]{:S(2)}, u32[]{:S(2)}) %all-to-all-start.1) | async-done | bytes 196640 | tf_op jit(solution)/shard_map/all_to_all | solution.py:61
  163.2 0.8 gather_fusion.1
  164.1 0.2 reshape.156
  164.3 0.4 multiply_reduce_fusion.1
  164.6 1.6 add_convert_fusion.1
  (19 shorter events, 0.1 us)
Async XLA Ops:
  6.5 52.9 %copy-start = (bf16[512,2048]{1,0:T(8,128)(2,1)S(1)}, bf16[512,2048]{1,0:T(8,128)(2,1)}, u32[]{:S(2)}) copy-start(bf16[512,2048]{1,0:T(8,128)(2,1)} %param.18) | copy-start | bytes 6291460
  6.5 41.7 %slice-start = ((bf16[64,4,192]{2,1,0:T(4,128)(2,1)}), bf16[64,4,64]{2,1,0:T(4,128)(2,1)S(1)}, s32[]{:S(2)}) async-start(bf16[64,4,192]{2,1,0:T(4,128)(2,1)} %param.13), calls=%async_computation.6 | async-start | bytes 131072 | tf_op jit(solution)/shard_map/slice | solution.py:85
  6.5 39.8 %copy-start.3 = (s32[64,2]{0,1:T(2,128)S(1)}, s32[64,2]{0,1:T(2,128)}, u32[]{:S(2)}) copy-start(s32[64,2]{0,1:T(2,128)} %param.21) | copy-start | bytes 1540
  6.5 47.7 %all-gather.2.cloned.1.call-start = ((), (), s32[]{:S(2)}) async-start(), calls=%async_computation.3 | async-start | bytes 1179648 | tf_op jit(solution)/shard_map/all_gather | solution.py:100
  11.0 80.7 %all-reduce.2.cloned.1.call-start = ((), (), s32[]{:S(2)}) async-start(), calls=%async_computation.4 | async-start | bytes 524288 | tf_op jit(solution)/shard_map/psum | solution.py:120
  56.1 35.6 %copy-start.1 = (bf16[64,2048]{1,0:T(8,128)(2,1)S(1)}, bf16[64,2048]{1,0:T(8,128)(2,1)}, u32[]{:S(2)}) copy-start(bf16[64,2048]{1,0:T(8,128)(2,1)} %param.19) | copy-start | bytes 786436
  56.5 37.2 %copy-start.2 = (f32[2048]{0:T(1024)S(1)}, f32[2048]{0:T(1024)}, u32[]{:S(2)}) copy-start(f32[2048]{0:T(1024)} %param.20) | copy-start | bytes 24580
  60.6 89.3 %reduce-scatter.2.cloned.1.call-start = ((), (), s32[]{:S(2)}) async-start(), calls=%async_computation.5 | async-start | bytes 983040 | tf_op jit(solution)/shard_map/reduce_scatter | solution.py:58
  95.9 27.9 %copy-start.5 = (bf16[1,2048,1024]{2,1,0:T(8,128)(2,1)S(1)}, bf16[1,2048,1024]{2,1,0:T(8,128)(2,1)}, u32[]{:S(2)}) copy-start(bf16[1,2048,1024]{2,1,0:T(8,128)(2,1)} %param.24) | copy-start | bytes 12582916
  123.8 2.2 %copy-start.6 = (bf16[1,1024,2048]{2,1,0:T(8,128)(2,1)S(1)}, bf16[1,1024,2048]{2,1,0:T(8,128)(2,1)}, u32[]{:S(2)}) copy-start(bf16[1,1024,2048]{2,1,0:T(8,128)(2,1)} %param.25) | copy-start | bytes 12582916
  124.9 30.5 %copy-start.4 = (f32[64,2]{0,1:T(2,128)S(1)}, f32[64,2]{0,1:T(2,128)}, u32[]{:S(2)}) copy-start(f32[64,2]{0,1:T(2,128)} %param.22) | copy-start | bytes 1540
  149.9 13.3 %all-to-all-start.1 = ((bf16[8,24,512]{2,1,0:T(8,128)(2,1)}), bf16[8,24,512]{2,1,0:T(8,128)(2,1)S(1)}, u32[]{:S(2)}, u32[]{:S(2)}) async-start(bf16[8,24,512]{2,1,0:T(8,128)(2,1)} %reduce-scatter.2.cloned.1.call-done), calls=%async_computation.2 | async-start | bytes 393216 | tf_op jit(solution)/shard_map/all_to_all | solution.py:61
Sparse Core Ops, SparseCore 0:
  11.2 43.0 all-gather.1
  60.8 30.9 all-reduce.1
  128.1 21.7 reduce-scatter.1
where the time goes:
time: 173 us
  waiting for transfers between devices  64.8 us (37%)
  blocking collectives  57.1 us (33%)
  between operations  13.4 us (8%)
  local copies, waits for them, and re-layouts  12.1 us (7%)
  matrix products  11.2 us (6%)
  other arithmetic  8.52 us (5%)
  starting transfers between devices  5.6 us (3%)
    all_gather x1, blocking collectives, shards(): turned_piece = lax.all_gather(turned_pairs, 'sp', axis=0, tiled=True)  32.5 us
    psum x1, waiting for transfers between devices, shards(): lax.psum(head_partial.astype(jnp.bfloat16), 'tp').astype(jnp.float32)  29.9 us
    all_to_all x1, blocking collectives, shards(): lax.all_to_all(outgoing, 'sp', split_axis=0, concat_axis=0, tiled=True)  24.6 us
    reduce_scatter x1, waiting for transfers between devices, finish_expert(): lax.psum_scatter(partial_rows.astype(jnp.bfloat16), 'tp', scatter_dimensi...  22 us
    all_to_all x1, waiting for transfers between devices, finish_expert(): lax.all_to_all(col_share, 'sp', split_axis=0, concat_axis=0, tiled=True)  7.68 us
    all_to_all x1, starting transfers between devices, finish_expert(): lax.all_to_all(col_share, 'sp', split_axis=0, concat_axis=0, tiled=True)  5.52 us
    all_gather x1, waiting for transfers between devices, shards(): lax.all_gather(own_projected.reshape(pair_rows, -1), 'sp', axis=0, tiled=...  5.2 us
  transfers between devices with their start and end apart: 4, of which 4 were waited for; matrix products, arithmetic and copies ran while one was open for 4% of the time, Pallas kernels for 0%

commit v1 on v0

--- a/solution.py
+++ b/solution.py
@@ -117,7 +117,9 @@
     head_partial = jnp.dot(
         attended.reshape(tok_rows, -1), out_weight, preferred_element_type=jnp.float32
     )
-    mixed = lax.psum(head_partial.astype(jnp.bfloat16), "tp").astype(jnp.float32)
+    mixed = jnp.sum(lax.all_gather(head_partial.astype(jnp.bfloat16), "tp"), axis=0).astype(
+        jnp.float32
+    )
     middle_float = (resid.astype(jnp.float32) + mixed).astype(jnp.bfloat16).astype(jnp.float32)
     normed = rms_scaled(middle_float, ffn_gain).astype(jnp.bfloat16)
     experts = lax.axis_size("sp")

time: 173 us -> 157 us (0.908)
  waiting for transfers between devices: 64.8 us -> 51.1 us
    psum x1 -> x0, waiting for transfers between devices: 29.9 us -> none  [shards(): lax.psum(head_partial.astype(jnp.bfloat16), 'tp').astype(jnp.float32)]
    all_gather x0 -> x1, waiting for transfers between devices: none -> 12.5 us  [shards(): lax.all_gather(head_partial.astype(jnp.bfloat16), 'tp')]
    all_gather x1, waiting for transfers between devices: 5.2 us -> 9.4 us  [shards(): lax.all_gather(own_projected.reshape(pair_rows, -1), 'sp', axis=0, tiled=...]
  transfers between devices with their start and end apart: 4 -> 4, of which waited for: 4 -> 4; matrix products, arithmetic and copies ran while one was open for 4% -> 3% of each run, Pallas kernels for 0% -> 0%
where the time goes in v1:
time: 157 us; the launch traced here: 156 us
  blocking collectives  58.5 us (37%)
  waiting for transfers between devices  51.1 us (33%)
  between operations  13.5 us (9%)
  local copies, waits for them, and re-layouts  10.6 us (7%)
  matrix products  9.52 us (6%)
  other arithmetic  7.42 us (5%)
  starting transfers between devices  5.6 us (4%)
    all_gather x1, blocking collectives, shards(): turned_piece = lax.all_gather(turned_pairs, 'sp', axis=0, tiled=True)  32.4 us
    all_to_all x1, blocking collectives, shards(): lax.all_to_all(outgoing, 'sp', split_axis=0, concat_axis=0, tiled=True)  26.1 us
    reduce_scatter x1, waiting for transfers between devices, finish_expert(): lax.psum_scatter(partial_rows.astype(jnp.bfloat16), 'tp', scatter_dimensi...  21.5 us
    all_gather x1, waiting for transfers between devices, shards(): lax.all_gather(head_partial.astype(jnp.bfloat16), 'tp')  12.5 us
    all_gather x1, waiting for transfers between devices, shards(): lax.all_gather(own_projected.reshape(pair_rows, -1), 'sp', axis=0, tiled=...  9.4 us
    all_to_all x1, waiting for transfers between devices, finish_expert(): lax.all_to_all(col_share, 'sp', split_axis=0, concat_axis=0, tiled=True)  7.68 us
    all_to_all x1, starting transfers between devices, finish_expert(): lax.all_to_all(col_share, 'sp', split_axis=0, concat_axis=0, tiled=True)  5.51 us
    dot_general x1, matrix products, shards(): jnp.dot(rows_in, gate_weight[0], preferred_element_type=jnp.float32)  3.2 us
  transfers between devices with their start and end apart: 4, of which 4 were waited for; matrix products, arithmetic and copies ran while one was open for 3% of the time, Pallas kernels for 0%

profile of v1, /device:TPU:0, one launch (start us, length us, event | category | flops | bytes accessed | tf_op | source)
XLA Modules:
  0.0 156.2 jit_solution(10116158458303477172)
XLA Ops:
  6.5 0.0 copy-start
  6.5 1.6 %copy.35 = bf16[64,8,4,256]{3,1,2,0:T(8,128)(2,1)S(1)} copy(bf16[64,8,4,256]{3,2,1,0:T(4,128)(2,1)} %bitcast.74) | data formatting | bytes 2097152
  8.1 0.0 slice-start.1
  8.2 1.0 fusion.28
  9.2 1.2 convolution_convert_fusion.1
  10.4 0.7 reshape.151
  11.0 0.0 all-gather.4.cloned.1.call-update
  11.1 0.0 all-gather.6.cloned.1.call-start
  11.1 0.7 convert_element_type.77
  11.9 0.2 multiply_cosine_fusion
  12.1 0.1 pad_maximum_fusion
  12.2 0.1 convert_element_type.79
  12.2 32.4 %all_gather.13 = bf16[256,128]{1,0:T(8,128)(2,1)S(1)} all-gather(bf16[32,128]{1,0:T(8,128)(2,1)S(1)} %convert_element_type.79), channel_id=1, replica_groups=mesh['sp'=8,'tp'=4] {'sp'}, dimensions={0}, use_global_device_ids=true | all-gather | bytes 73728 | tf_op jit(solution)/shard_map/all_gather | solution.py:101
  44.6 0.1 reshape.152
  44.8 0.1 subtract_convert_fusion
  44.9 9.4 %all-gather.4.cloned.1.call-done = bf16[256,2048]{1,0:T(8,128)(2,1)} async-done(((bf16[32,2048]{1,0:T(8,128)(2,1)}), bf16[256,2048]{1,0:T(8,128)(2,1)}) %all-gather.4.cloned.1.call-update) | async-done | bytes 1048592 | tf_op jit(solution)/shard_map/all_gather | solution.py:100
  54.3 1.8 %reshape_reshape.3 = bf16[512,4,256]{2,1,0:T(4,128)(2,1)S(1)} reshape(bf16[256,2048]{1,0:T(8,128)(2,1)} %all-gather.4.cloned.1.call-done) | data formatting | bytes 2097152 | tf_op jit(solution)/shard_map/reshape;reshape | solution.py:104
  56.1 0.0 copy-start.3
  56.1 0.4 fusion.48
  56.5 0.0 slice-done.1
  56.5 0.0 copy-start.1
  56.5 0.3 convolution_bitcast_fusion.1
  56.8 0.0 copy-start.2
  56.9 0.4 fusion.49
  57.2 0.2 fusion.23
  57.5 0.3 fusion.20
  57.8 1.2 convolution_convert_fusion
  59.0 0.0 all-gather.6.cloned.1.call-update
  59.0 0.0 reduce-scatter.2.cloned.1.call-start
  59.1 0.1 copy.26
  59.2 0.1 eq.15
  59.3 0.1 copy.25
  59.4 0.1 mul.175
  59.6 0.1 fusion.39
  59.6 0.2 reduce_window_sum.11
  59.8 0.2 select_reduce_fusion
  60.0 1.0 scatter_custom_fusion.1
  61.0 1.0 scatter_custom_fusion
  62.0 0.1 broadcast_in_dim.24
  62.1 12.5 %all-gather.6.cloned.1.call-done = bf16[256,2048]{1,0:T(8,128)(2,1)} async-done(((bf16[64,2048]{1,0:T(8,128)(2,1)}), bf16[256,2048]{1,0:T(8,128)(2,1)}) %all-gather.6.cloned.1.call-update) | async-done | bytes 1048592 | tf_op jit(solution)/shard_map/all_gather | solution.py:120
  74.6 1.4 reduce_sum.64
  76.0 1.0 fusion.26
  77.1 0.1 multiply_convert_fusion
  77.2 1.1 gather_fusion
  78.3 0.0 copy-start.5
  78.3 0.1 broadcast_select_fusion
  78.5 26.1 %all_to_all.10 = bf16[8,24,2048]{2,1,0:T(8,128)(2,1)S(1)} all-to-all(bf16[8,24,2048]{2,1,0:T(8,128)(2,1)S(1)} %broadcast_select_fusion), channel_id=1, replica_groups=mesh['sp'=8,'tp'=4] {'sp'}, dimensions={0} | all-to-all | bytes 1572864 | tf_op jit(solution)/shard_map/all_to_all | solution.py:138
  104.5 3.2 %fusion.4 = f32[192,1024]{1,0:T(8,128)S(1)} fusion(bf16[192,2048]{1,0:T(8,128)(2,1)S(1)} %bitcast.70, bf16[1,2048,1024]{2,1,0:T(8,128)(2,1)} %param.23), kind=kOutput, calls=%fused_computation.8 | convolution fusion | flops 805306368 | bytes 5767168 | tf_op jit(solution)/shard_map/dot_general | solution.py:141
  107.7 0.0 copy-done.5
  107.8 0.0 copy-start.6
  107.8 1.1 fusion.12
  108.8 0.0 copy-start.4
  108.9 1.1 copy-done.6
  109.9 1.9 %fusion.6 = bf16[8,24,2048]{2,1,0:T(8,128)(2,1)} fusion(bf16[8,24,1024]{2,1,0:T(8,128)(2,1)S(1)} %bitcast.75, bf16[1,1024,2048]{2,1,0:T(8,128)(2,1)S(1)} %copy-done.6), kind=kOutput, calls=%fused_computation.10 | convolution fusion | flops 805699584 | bytes 5373952 | tf_op jit(solution)/shard_map/dot_general | solution.py:55
  111.9 0.0 reduce-scatter.2.cloned.1.call-update
  111.9 21.5 %reduce-scatter.2.cloned.1.call-done = bf16[8,24,512]{2,1,0:T(8,128)(2,1)} async-done(((bf16[8,24,2048]{2,1,0:T(8,128)(2,1)}), bf16[8,24,512]{2,1,0:T(8,128)(2,1)}) %reduce-scatter.2.cloned.1.call-update) | async-done | bytes 196624 | tf_op jit(solution)/shard_map/reduce_scatter | solution.py:58
  133.4 5.5 %all-to-all-start.1 = ((bf16[8,24,512]{2,1,0:T(8,128)(2,1)}), bf16[8,24,512]{2,1,0:T(8,128)(2,1)S(1)}, u32[]{:S(2)}, u32[]{:S(2)}) async-start(bf16[8,24,512]{2,1,0:T(8,128)(2,1)} %reduce-scatter.2.cloned.1.call-done), calls=%async_computation.2 | async-start | bytes 393216 | tf_op jit(solution)/shard_map/all_to_all | solution.py:61
  138.9 0.0 copy-done.4
  138.9 0.1 copy.27
  139.0 7.7 %all-to-all-done.1 = bf16[8,24,512]{2,1,0:T(8,128)(2,1)S(1)} async-done(((bf16[8,24,512]{2,1,0:T(8,128)(2,1)}), bf16[8,24,512]{2,1,0:T(8,128)(2,1)S(1)}, u32[]{:S(2)}, u32[]{:S(2)}) %all-to-all-start.1) | async-done | bytes 196640 | tf_op jit(solution)/shard_map/all_to_all | solution.py:61
  146.7 0.8 gather_fusion.1
  147.5 0.2 reshape.156
  147.7 0.4 multiply_reduce_fusion.1
  148.1 1.6 %add_convert_fusion.1 = bf16[64,512]{1,0:T(8,128)(2,1)} fusion(f32[64,512]{1,0:T(8,128)S(1)} %multiply_reduce_fusion.1, f32[64,2048]{1,0:T(8,128)} %get-tuple-element.7, s32[]{:T(128)S(6)} %select_n.28), kind=kLoop, calls=%fused_computation.42 | loop fusion | flops 65536 | bytes 327684 | tf_op jit(solution)/shard_map/convert_element_type | solution.py:150
  (21 shorter events, 0.1 us)
Async XLA Ops:
  6.5 51.2 %copy-start = (bf16[512,2048]{1,0:T(8,128)(2,1)S(1)}, bf16[512,2048]{1,0:T(8,128)(2,1)}, u32[]{:S(2)}) copy-start(bf16[512,2048]{1,0:T(8,128)(2,1)} %param.18) | copy-start | bytes 6291460
  6.5 38.2 %slice-start = ((bf16[64,4,192]{2,1,0:T(4,128)(2,1)}), bf16[64,4,64]{2,1,0:T(4,128)(2,1)S(1)}, s32[]{:S(2)}) async-start(bf16[64,4,192]{2,1,0:T(4,128)(2,1)} %param.13), calls=%async_computation.6 | async-start | bytes 131072 | tf_op jit(solution)/shard_map/slice | solution.py:85
  6.5 47.7 %all-gather.4.cloned.1.call-start = ((), (), s32[]{:S(2)}) async-start(), calls=%async_computation.3 | async-start | bytes 1179648 | tf_op jit(solution)/shard_map/all_gather | solution.py:100
  8.1 48.4 %slice-start.1 = ((bf16[64,4,192]{2,1,0:T(4,128)(2,1)}), bf16[64,4,128]{2,1,0:T(4,128)(2,1)S(1)}, s32[]{:S(2)}) async-start(bf16[64,4,192]{2,1,0:T(4,128)(2,1)} %param.13), calls=%async_computation.7 | async-start | bytes 131072 | tf_op jit(solution)/shard_map/slice | solution.py:83
  11.1 63.6 %all-gather.6.cloned.1.call-start = ((), (), s32[]{:S(2)}) async-start(), calls=%async_computation.5 | async-start | bytes 1310720 | tf_op jit(solution)/shard_map/all_gather | solution.py:120
  56.1 2.9 %copy-start.3 = (s32[64,2]{0,1:T(2,128)S(1)}, s32[64,2]{0,1:T(2,128)}, u32[]{:S(2)}) copy-start(s32[64,2]{0,1:T(2,128)} %param.21) | copy-start | bytes 1540
  56.5 19.5 %copy-start.1 = (bf16[64,2048]{1,0:T(8,128)(2,1)S(1)}, bf16[64,2048]{1,0:T(8,128)(2,1)}, u32[]{:S(2)}) copy-start(bf16[64,2048]{1,0:T(8,128)(2,1)} %param.19) | copy-start | bytes 786436
  56.8 20.2 %copy-start.2 = (f32[2048]{0:T(1024)S(1)}, f32[2048]{0:T(1024)}, u32[]{:S(2)}) copy-start(f32[2048]{0:T(1024)} %param.20) | copy-start | bytes 24580
  59.0 74.4 %reduce-scatter.2.cloned.1.call-start = ((), (), s32[]{:S(2)}) async-start(), calls=%async_computation.4 | async-start | bytes 983040 | tf_op jit(solution)/shard_map/reduce_scatter | solution.py:58
  78.3 29.4 %copy-start.5 = (bf16[1,2048,1024]{2,1,0:T(8,128)(2,1)S(1)}, bf16[1,2048,1024]{2,1,0:T(8,128)(2,1)}, u32[]{:S(2)}) copy-start(bf16[1,2048,1024]{2,1,0:T(8,128)(2,1)} %param.24) | copy-start | bytes 12582916
  107.8 2.2 %copy-start.6 = (bf16[1,1024,2048]{2,1,0:T(8,128)(2,1)S(1)}, bf16[1,1024,2048]{2,1,0:T(8,128)(2,1)}, u32[]{:S(2)}) copy-start(bf16[1,1024,2048]{2,1,0:T(8,128)(2,1)} %param.25) | copy-start | bytes 12582916
  108.8 30.0 %copy-start.4 = (f32[64,2]{0,1:T(2,128)S(1)}, f32[64,2]{0,1:T(2,128)}, u32[]{:S(2)}) copy-start(f32[64,2]{0,1:T(2,128)} %param.22) | copy-start | bytes 1540
  133.4 13.3 %all-to-all-start.1 = ((bf16[8,24,512]{2,1,0:T(8,128)(2,1)}), bf16[8,24,512]{2,1,0:T(8,128)(2,1)S(1)}, u32[]{:S(2)}, u32[]{:S(2)}) async-start(bf16[8,24,512]{2,1,0:T(8,128)(2,1)} %reduce-scatter.2.cloned.1.call-done), calls=%async_computation.2 | async-start | bytes 393216 | tf_op jit(solution)/shard_map/all_to_all | solution.py:61
Sparse Core Ops, SparseCore 0:
  11.2 43.0 all-gather.3
  59.1 15.4 all-gather.5
  112.0 21.3 reduce-scatter.1
